TPU v7x, 32 devices: a whole 2x2x4 slice. The times are simulated.
32 devices in a mesh: fs: 8 (over z, x), tp: 4 (over y, core).
Axes of the slice: x: 2, y: 2, z: 4, core: 2. Of those that a mesh axis runs over, the one named last changes fastest.
Arguments:
- tokens: bfloat16 [4096, 2048], P(('fs', 'tp')), may hold values from -6 to 6
- gate_weight: bfloat16 [5632, 2048], P('tp', 'fs'), may hold values from -0.125 to 0.125
- up_weight: bfloat16 [5632, 2048], P('tp', 'fs'), may hold values from -0.125 to 0.125
- down_weight: bfloat16 [5632, 2048], P('tp', 'fs'), may hold values from -0.078125 to 0.078125
- out_grad: bfloat16 [4096, 2048], P(('fs', 'tp')), may hold values from -6 to 6
Outputs:
- grad_tokens: bfloat16 [4096, 2048], P(('fs', 'tp'))
- grad_gate: float32 [5632, 2048], P('tp', 'fs')
- grad_up: float32 [5632, 2048], P('tp', 'fs')
- grad_down: float32 [5632, 2048], P('tp', 'fs')
- gate_rows: float32 [5632], P('tp')
- up_rows: float32 [5632], P('tp')
- down_rows: float32 [5632], P('tp')
All inputs are finite; a program needn't handle non-finite values.
Results may differ from a plain program's by a relative error of at most 0.014.
Values may be sent and summed in bfloat16 or wider, within the bound.
A program may use at most 128 MiB of HBM per device.

v0:
```python
import math
import jax
import jax.numpy as jnp
from jax import lax
from jax.sharding import PartitionSpec as P


def body(tokens, gate_weight, up_weight, down_weight, out_grad):
    inputs, cotangent = (
        lax.all_gather(tokens, "tp", axis=0, tiled=True),
        lax.all_gather(out_grad, "tp", axis=0, tiled=True),
    )
    w_gate, w_up, w_down = (
        lax.all_gather(gate_weight, "fs", axis=1, tiled=True),
        lax.all_gather(up_weight, "fs", axis=1, tiled=True),
        lax.all_gather(down_weight, "fs", axis=1, tiled=True),
    )
    inner = (((1,), (1,)), ((), ()))
    gate = lax.dot_general(inputs, w_gate, inner, preferred_element_type=jnp.float32)
    up = lax.dot_general(inputs, w_up, inner, preferred_element_type=jnp.float32)
    dhidden = lax.dot_general(cotangent, w_down, inner, preferred_element_type=jnp.float32)
    sig = jax.nn.sigmoid(gate)
    silu = gate * sig
    act = (silu * up).astype(jnp.bfloat16)
    dgate = (dhidden * up * sig * (1.0 + gate * (1.0 - sig))).astype(jnp.bfloat16)
    dup = (dhidden * silu).astype(jnp.bfloat16)
    term = jnp.dot(dgate, w_gate, preferred_element_type=jnp.float32)
    grad_tokens = lax.psum_scatter(
        (term + jnp.dot(dup, w_up, preferred_element_type=jnp.float32)).astype(jnp.bfloat16),
        "tp",
        scatter_dimension=0,
        tiled=True,
    )
    factor = 1.0 / math.sqrt(inputs.shape[0] * lax.axis_size("fs"))
    outer = (((0,), (0,)), ((), ()))
    width = gate_weight.shape[1] * lax.axis_size("fs")
    part_gate = lax.dot_general(dgate, inputs, outer, preferred_element_type=jnp.float32) * factor
    part_up = lax.dot_general(dup, inputs, outer, preferred_element_type=jnp.float32) * factor
    part_down = lax.dot_general(act, cotangent, outer, preferred_element_type=jnp.float32) * factor
    grad_gate, grad_up, grad_down = (
        lax.psum_scatter(
            part_gate.astype(jnp.bfloat16), "fs", scatter_dimension=1, tiled=True
        ).astype(jnp.float32),
        lax.psum_scatter(
            part_up.astype(jnp.bfloat16), "fs", scatter_dimension=1, tiled=True
        ).astype(jnp.float32),
        lax.psum_scatter(
            part_down.astype(jnp.bfloat16), "fs", scatter_dimension=1, tiled=True
        ).astype(jnp.float32),
    )
    sums = lax.psum(
        (
            jnp.sum(grad_gate * grad_gate, axis=1),
            jnp.sum(grad_up * grad_up, axis=1),
            jnp.sum(grad_down * grad_down, axis=1),
        ),
        "fs",
    )
    gate_rows, up_rows, down_rows = (sums[0] / width, sums[1] / width, sums[2] / width)
    return (grad_tokens, grad_gate, grad_up, grad_down, gate_rows, up_rows, down_rows)


def solution(mesh):
    return jax.shard_map(
        body,
        mesh=mesh,
        in_specs=(
            P(("fs", "tp"), None),
            P("tp", "fs"),
            P("tp", "fs"),
            P("tp", "fs"),
            P(("fs", "tp"), None),
        ),
        out_specs=(
            P(("fs", "tp"), None),
            P("tp", "fs"),
            P("tp", "fs"),
            P("tp", "fs"),
            P("tp"),
            P("tp"),
            P("tp"),
        ),
        check_vma=False,
    )
```

profile of v0, /device:TPU:0, one launch (start us, length us, event | category | flops | bytes accessed | tf_op | source)
XLA Modules:
  0.0 727.2 jit_solution(359217630501200977)
XLA Ops:
  7.2 0.7 all-gather.10.cloned.1.call-update
  7.9 0.7 all-gather.12.cloned.1.call-update
  8.7 0.7 all-gather.14.cloned.1.call-update
  10.6 24.3 %all-gather.10.cloned.1.call-done = bf16[512,2048]{1,0:T(8,128)(2,1)} async-done(((bf16[128,2048]{1,0:T(8,128)(2,1)}), bf16[512,2048]{1,0:T(8,128)(2,1)}) %all-gather.10.cloned.1.call-update) | async-done | bytes 2097168 | tf_op jit(solution)/shard_map/all_gather | solution.py:10
  34.9 95.2 %all-gather.12.cloned.1.call-done = bf16[1408,2048]{1,0:T(8,128)(2,1)} async-done(((bf16[1408,256]{1,0:T(8,128)(2,1)}), bf16[1408,2048]{1,0:T(8,128)(2,1)}) %all-gather.12.cloned.1.call-update) | async-done | bytes 5767184 | tf_op jit(solution)/shard_map/all_gather | solution.py:15
  130.1 8.3 %fusion.3 = f32[512,1408]{1,0:T(8,128)} fusion(bf16[512,2048]{1,0:T(8,128)(2,1)} %all-gather.10.cloned.1.call-done, bf16[1408,2048]{1,0:T(8,128)(2,1)} %all-gather.12.cloned.1.call-done), kind=kOutput, calls=%fused_computation.16 | convolution fusion | flops 2952790016 | bytes 10747904 | tf_op jit(solution)/shard_map/dot_general | solution.py:20
  138.4 85.1 %all-gather.14.cloned.1.call-done = bf16[1408,2048]{1,0:T(8,128)(2,1)} async-done(((bf16[1408,256]{1,0:T(8,128)(2,1)}), bf16[1408,2048]{1,0:T(8,128)(2,1)}) %all-gather.14.cloned.1.call-update) | async-done | bytes 5767184 | tf_op jit(solution)/shard_map/all_gather | solution.py:14
  223.5 7.6 %fusion.4 = f32[512,1408]{1,0:T(8,128)} fusion(bf16[512,2048]{1,0:T(8,128)(2,1)S(1)} %copy-done, bf16[1408,2048]{1,0:T(8,128)(2,1)} %all-gather.14.cloned.1.call-done), kind=kOutput, calls=%fused_computation.17 | convolution fusion | flops 2952790016 | bytes 10747904 | tf_op jit(solution)/shard_map/dot_general | solution.py:19
  231.1 14.6 %all-gather.6.cloned.1.call-done = bf16[512,2048]{1,0:T(8,128)(2,1)} async-done(((bf16[128,2048]{1,0:T(8,128)(2,1)}), bf16[512,2048]{1,0:T(8,128)(2,1)}) %all-gather.6.cloned.1.call-update) | async-done | bytes 2097168 | tf_op jit(solution)/shard_map/all_gather | solution.py:11
  245.7 9.1 %multiply_convert_fusion = bf16[1408,2048]{1,0:T(8,128)(2,1)} fusion(bf16[512,2048]{1,0:T(8,128)(2,1)} %all-gather.6.cloned.1.call-done, f32[512,1408]{1,0:T(8,128)} %fusion.3, f32[512,1408]{1,0:T(8,128)} %fusion.4), kind=kOutput, calls=%fused_computation | convolution fusion | flops 2962882560 | bytes 13631488 | tf_op jit(solution)/shard_map/dot_general | solution.py:39
  255.0 85.7 %all-gather.8.cloned.1.call-done = bf16[1408,2048]{1,0:T(8,128)(2,1)} async-done(((bf16[1408,256]{1,0:T(8,128)(2,1)}), bf16[1408,2048]{1,0:T(8,128)(2,1)}) %all-gather.8.cloned.1.call-update) | async-done | bytes 5767184 | tf_op jit(solution)/shard_map/all_gather | solution.py:16
  340.7 10.2 %multiply_convert_fusion.4 = (bf16[512,1408]{1,0:T(8,128)(2,1)S(1)}, bf16[512,1408]{1,0:T(8,128)(2,1)}) fusion(f32[512,1408]{1,0:T(8,128)} %fusion.4, f32[512,1408]{1,0:T(8,128)} %fusion.3, bf16[512,2048]{1,0:T(8,128)(2,1)} %all-gather.6.cloned.1.call-done, bf16[1408,2048]{1,0:T(8,128)(2,1)} %all-gather.8.cloned.1.call-done), kind=kOutput, calls=%fused_computation.5 | convolution fusion | flops 2962161664 | bytes 16515072 | tf_op jit(solution)/shard_map/dot_general | solution.py:21
  350.9 5.0 multiply_convert_fusion.1
  355.9 6.5 multiply_convert_fusion.2
  362.5 1.3 copy-done.1
  363.8 5.4 fusion.5
  369.2 7.4 %add_convert_fusion = bf16[512,2048]{1,0:T(8,128)(2,1)} fusion(f32[512,2048]{1,0:T(8,128)S(1)} %fusion.5, bf16[512,1408]{1,0:T(8,128)(2,1)S(1)} %get-tuple-element.16, bf16[1408,2048]{1,0:T(8,128)(2,1)} %all-gather.12.cloned.1.call-done), kind=kOutput, calls=%fused_computation.3 | convolution fusion | flops 2954887168 | bytes 13500416 | tf_op jit(solution)/shard_map/dot_general | solution.py:29
  376.6 76.8 %reduce-scatter.11.cloned.1.call-done = bf16[1408,256]{1,0:T(8,128)(2,1)} async-done(((bf16[1408,2048]{1,0:T(8,128)(2,1)}), bf16[1408,256]{1,0:T(8,128)(2,1)}) %reduce-scatter.11.cloned.1.call-update) | async-done | bytes 720912 | tf_op jit(solution)/shard_map/reduce_scatter | solution.py:47
  453.5 2.3 multiply_reduce_fusion
  455.8 111.8 %reduce-scatter.9.cloned.1.call-done = bf16[1408,256]{1,0:T(8,128)(2,1)} async-done(((bf16[1408,2048]{1,0:T(8,128)(2,1)}), bf16[1408,256]{1,0:T(8,128)(2,1)}) %reduce-scatter.9.cloned.1.call-update) | async-done | bytes 720912 | tf_op jit(solution)/shard_map/reduce_scatter | solution.py:44
  567.6 2.3 multiply_reduce_fusion.1
  569.9 111.8 %reduce-scatter.7.cloned.1.call-done = bf16[1408,256]{1,0:T(8,128)(2,1)} async-done(((bf16[1408,2048]{1,0:T(8,128)(2,1)}), bf16[1408,256]{1,0:T(8,128)(2,1)}) %reduce-scatter.7.cloned.1.call-update) | async-done | bytes 720912 | tf_op jit(solution)/shard_map/reduce_scatter | solution.py:41
  681.7 2.3 multiply_reduce_fusion.2
  684.0 35.5 %all-reduce = (f32[1408]{0:T(1024)S(1)}, f32[1408]{0:T(1024)S(1)}, f32[1408]{0:T(1024)S(1)}) all-reduce(f32[1408]{0:T(1024)S(1)} %get-tuple-element.14, f32[1408]{0:T(1024)S(1)} %get-tuple-element.12, f32[1408]{0:T(1024)S(1)} %get-tuple-element.10), channel_id=1, replica_groups=mesh['fs'=8,'tp'=4] {'fs'}, use_global_device_ids=true, to_apply=%region_5.0 | all-reduce | flops 4224 | bytes 33792 | tf_op jit(solution)/shard_map/psum | solution.py:51
  (21 shorter events, 2.9 us)
Async XLA Ops:
  7.2 27.7 %all-gather.10.cloned.1.call-start = ((), (), s32[]{:S(2)}) async-start(), calls=%async_computation.6 | async-start | bytes 2621440 | tf_op jit(solution)/shard_map/all_gather | solution.py:10
  7.9 122.2 %all-gather.12.cloned.1.call-start = ((), (), s32[]{:S(2)}) async-start(), calls=%async_computation.7 | async-start | bytes 6488064 | tf_op jit(solution)/shard_map/all_gather | solution.py:15
  8.6 214.8 %all-gather.14.cloned.1.call-start = ((), (), s32[]{:S(2)}) async-start(), calls=%async_computation.8 | async-start | bytes 6488064 | tf_op jit(solution)/shard_map/all_gather | solution.py:14
  9.4 236.3 %all-gather.6.cloned.1.call-start = ((), (), s32[]{:S(2)}) async-start(), calls=%async_computation.4 | async-start | bytes 2621440 | tf_op jit(solution)/shard_map/all_gather | solution.py:11
  10.0 330.7 %all-gather.8.cloned.1.call-start = ((), (), s32[]{:S(2)}) async-start(), calls=%async_computation.5 | async-start | bytes 6488064 | tf_op jit(solution)/shard_map/all_gather | solution.py:16
  10.5 442.9 %reduce-scatter.11.cloned.1.call-start = ((), (), s32[]{:S(2)}) async-start(), calls=%async_computation.12 | async-start | bytes 6488064 | tf_op jit(solution)/shard_map/reduce_scatter | solution.py:47
  34.9 188.6 %copy-start = (bf16[512,2048]{1,0:T(8,128)(2,1)S(1)}, bf16[512,2048]{1,0:T(8,128)(2,1)}, u32[]{:S(2)}) copy-start(bf16[512,2048]{1,0:T(8,128)(2,1)} %all-gather.10.cloned.1.call-done) | copy-start | bytes 6291460
  254.7 312.8 %reduce-scatter.9.cloned.1.call-start = ((), (), s32[]{:S(2)}) async-start(), calls=%async_computation.11 | async-start | bytes 6488064 | tf_op jit(solution)/shard_map/reduce_scatter | solution.py:44
  355.9 325.8 %reduce-scatter.7.cloned.1.call-start = ((), (), s32[]{:S(2)}) async-start(), calls=%async_computation.10 | async-start | bytes 6488064 | tf_op jit(solution)/shard_map/reduce_scatter | solution.py:41
  362.4 1.4 copy-start.1
  362.4 358.3 %reduce-scatter.5.cloned.1.call-start = ((), (), s32[]{:S(2)}) async-start(), calls=%async_computation.9 | async-start | bytes 2621440 | tf_op jit(solution)/shard_map/reduce_scatter | solution.py:28
Sparse Core Ops, SparseCore 0:
  9.5 25.2 all-gather.9
  36.9 93.1 all-gather.11
  132.1 91.3 all-gather.13
  224.9 20.7 all-gather.5
  247.5 93.1 all-gather.7
  344.2 109.1 reduce-scatter.10
  457.1 110.3 reduce-scatter.8
  571.2 110.3 reduce-scatter.6
  684.8 30.5 reduce-scatter.4
where the time goes:
time: 728 us; the launch traced here: 727 us
  waiting for transfers between devices  608 us (84%)
  matrix products  59.5 us (8%)
  blocking collectives  35.5 us (5%)
  between operations  13.9 us (2%)
  other arithmetic  8.24 us (1%)
    reduce_scatter x1, waiting for transfers between devices, body(): lax.psum_scatter(part_up.astype(jnp.bfloat16), 'fs', scatter_dimension=1,...  112 us
    reduce_scatter x1, waiting for transfers between devices, body(): lax.psum_scatter(part_gate.astype(jnp.bfloat16), 'fs', scatter_dimension=...  112 us
    all_gather x1, waiting for transfers between devices, body(): lax.all_gather(up_weight, 'fs', axis=1, tiled=True)  95.2 us
    all_gather x1, waiting for transfers between devices, body(): lax.all_gather(down_weight, 'fs', axis=1, tiled=True)  85.7 us
    all_gather x1, waiting for transfers between devices, body(): lax.all_gather(gate_weight, 'fs', axis=1, tiled=True)  85.1 us
    reduce_scatter x1, waiting for transfers between devices, body(): lax.psum_scatter(part_down.astype(jnp.bfloat16), 'fs', scatter_dimension=...  76.8 us
    psum x1, blocking collectives, body(): lax.psum((jnp.sum(grad_gate * grad_gate, axis=1), jnp.sum(grad_up * grad_...  35.5 us
    all_gather x1, waiting for transfers between devices, body(): lax.all_gather(tokens, 'tp', axis=0, tiled=True)  24.3 us
  transfers between devices with their start and end apart: 9, of which 8 were waited for; matrix products, arithmetic and copies ran while one was open for 9% of the time, Pallas kernels for 0%

commit v1 on v0

--- a/solution.py
+++ b/solution.py
@@ -3,6 +3,22 @@
 import jax.numpy as jnp
 from jax import lax
 from jax.sharding import PartitionSpec as P
+
+
+def ring_gather(x, axis, dim):
+    ways, here, turn = (lax.axis_size(axis), lax.axis_index(axis), x.shape[dim])
+    dims = [n * ways if d == dim else n for d, n in enumerate(x.shape)]
+    full = lax.dynamic_update_slice_in_dim(jnp.zeros(dims, x.dtype), x, here * turn, axis=dim)
+    going_up = going_down = x
+    for far in range(1, ways // 2 + 1):
+        going_up = lax.ppermute(going_up, axis, [(d, (d + 1) % ways) for d in range(ways)])
+        full = lax.dynamic_update_slice_in_dim(full, going_up, (here - far) % ways * turn, axis=dim)
+        if 2 * far < ways:
+            going_down = lax.ppermute(going_down, axis, [(d, (d - 1) % ways) for d in range(ways)])
+            full = lax.dynamic_update_slice_in_dim(
+                full, going_down, (here + far) % ways * turn, axis=dim
+            )
+    return full
 
 
 def body(tokens, gate_weight, up_weight, down_weight, out_grad):
@@ -12,7 +28,7 @@
     )
     w_gate, w_up, w_down = (
         lax.all_gather(gate_weight, "fs", axis=1, tiled=True),
-        lax.all_gather(up_weight, "fs", axis=1, tiled=True),
+        ring_gather(up_weight, "fs", 1),
         lax.all_gather(down_weight, "fs", axis=1, tiled=True),
     )
     inner = (((1,), (1,)), ((), ()))

time: 728 us -> 702 us (0.964)
  waiting for transfers between devices: 608 us -> 553 us
  starting transfers between devices: 0.53 us -> 20 us
  local copies, waits for them, and re-layouts: 1.29 us -> 14.9 us
    ppermute x0 -> x7, waiting for transfers between devices: none -> 120 us  [the longest x4 120 us: ring_gather(): lax.ppermute(going_up, axis, [(d, (d + 1) % ways) for d in range(ways)])]
    all_gather x1 -> x0, waiting for transfers between devices: 95.2 us -> none  [body(): lax.all_gather(up_weight, 'fs', axis=1, tiled=True)]
    all_gather x1, waiting for transfers between devices: 85.1 us -> 17 us  [body(): lax.all_gather(gate_weight, 'fs', axis=1, tiled=True)]
    reduce_scatter x1, waiting for transfers between devices: 76.8 us -> 112 us  [body(): lax.psum_scatter(part_down.astype(jnp.bfloat16), 'fs', scatter_dimension=...]
    reduce_scatter x1, waiting for transfers between devices: 112 us -> 80.2 us  [body(): lax.psum_scatter(part_gate.astype(jnp.bfloat16), 'fs', scatter_dimension=...]
    all_gather x1, waiting for transfers between devices: 24.3 us -> 0.01 us  [body(): lax.all_gather(tokens, 'tp', axis=0, tiled=True)]
    ppermute x0 -> x7, starting transfers between devices: none -> 19.5 us  [the longest x4 10.4 us: ring_gather(): lax.ppermute(going_up, axis, [(d, (d + 1) % ways) for d in range(ways)])]
    all_gather x1, waiting for transfers between devices: 85.7 us -> 95.1 us  [body(): lax.all_gather(down_weight, 'fs', axis=1, tiled=True)]
  transfers between devices with their start and end apart: 9 -> 15, of which waited for: 8 -> 11; matrix products, arithmetic and copies ran while one was open for 9% -> 9% of each run, Pallas kernels for 0% -> 0%
where the time goes in v1:
time: 702 us
  waiting for transfers between devices  553 us (79%)
  matrix products  56 us (8%)
  blocking collectives  35.5 us (5%)
  starting transfers between devices  20 us (3%)
  local copies, waits for them, and re-layouts  14.9 us (2%)
  between operations  14.2 us (2%)
  other arithmetic  8.24 us (1%)
    ppermute x4, waiting for transfers between devices, ring_gather(): lax.ppermute(going_up, axis, [(d, (d + 1) % ways) for d in range(ways)])  120 us
    reduce_scatter x1, waiting for transfers between devices, body(): lax.psum_scatter(part_down.astype(jnp.bfloat16), 'fs', scatter_dimension=...  112 us
    reduce_scatter x1, waiting for transfers between devices, body(): lax.psum_scatter(part_up.astype(jnp.bfloat16), 'fs', scatter_dimension=1,...  112 us
    all_gather x1, waiting for transfers between devices, body(): lax.all_gather(down_weight, 'fs', axis=1, tiled=True)  95.1 us
    reduce_scatter x1, waiting for transfers between devices, body(): lax.psum_scatter(part_gate.astype(jnp.bfloat16), 'fs', scatter_dimension=...  80.2 us
    psum x1, blocking collectives, body(): lax.psum((jnp.sum(grad_gate * grad_gate, axis=1), jnp.sum(grad_up * grad_...  35.5 us
    all_gather x1, waiting for transfers between devices, body(): lax.all_gather(gate_weight, 'fs', axis=1, tiled=True)  17 us
    all_gather x1, waiting for transfers between devices, body(): lax.all_gather(out_grad, 'tp', axis=0, tiled=True)  14.6 us
  transfers between devices with their start and end apart: 15, of which 11 were waited for; matrix products, arithmetic and copies ran while one was open for 9% of the time, Pallas kernels for 0%

profile of v1, /device:TPU:0, one launch (start us, length us, event | category | flops | bytes accessed | tf_op | source)
XLA Modules:
  0.0 702.0 jit_solution(4587406221404183118)
XLA Ops:
  10.0 3.0 collective-permute-start
  13.0 3.1 collective-permute-start.1
  16.1 28.1 %collective-permute-done = bf16[1408,256]{1,0:T(8,128)(2,1)S(1)} collective-permute-done((bf16[1408,256]{1,0:T(8,128)(2,1)}, bf16[1408,256]{1,0:T(8,128)(2,1)S(1)}, u32[]{:S(2)}, u32[]{:S(2)}) %collective-permute-start) | collective-permute-done | bytes 720928 | tf_op jit(solution)/shard_map/ppermute | solution.py:14
  46.6 3.1 collective-permute-start.3
  49.7 3.2 broadcast_in_dim.3
  53.8 30.4 %collective-permute-done.2 = bf16[1408,256]{1,0:T(8,128)(2,1)S(1)} collective-permute-done((bf16[1408,256]{1,0:T(8,128)(2,1)S(1)}, bf16[1408,256]{1,0:T(8,128)(2,1)S(1)}, u32[]{:S(2)}, u32[]{:S(2)}) %collective-permute-start.2) | collective-permute-done | bytes 720928 | tf_op jit(solution)/shard_map/ppermute | solution.py:14
  88.6 3.0 collective-permute-start.5
  92.6 33.2 %collective-permute-done.4 = bf16[1408,256]{1,0:T(8,128)(2,1)S(1)} collective-permute-done((bf16[1408,256]{1,0:T(8,128)(2,1)S(1)}, bf16[1408,256]{1,0:T(8,128)(2,1)S(1)}, u32[]{:S(2)}, u32[]{:S(2)}) %collective-permute-start.4) | collective-permute-done | bytes 720928 | tf_op jit(solution)/shard_map/ppermute | solution.py:14
  132.0 27.9 %collective-permute-done.6 = bf16[1408,256]{1,0:T(8,128)(2,1)S(1)} collective-permute-done((bf16[1408,256]{1,0:T(8,128)(2,1)S(1)}, bf16[1408,256]{1,0:T(8,128)(2,1)S(1)}, u32[]{:S(2)}, u32[]{:S(2)}) %collective-permute-start.6) | collective-permute-done | bytes 720928 | tf_op jit(solution)/shard_map/ppermute | solution.py:14
  160.8 8.5 %convolution_bitcast_fusion = f32[512,1408]{1,0:T(8,128)} fusion(bf16[1408,2048]{1,0:T(8,128)(2,1)} %constant_dynamic-update-slice_fusion, bf16[512,2048]{1,0:T(8,128)(2,1)} %all-gather.9.cloned.1.call-done), kind=kOutput, calls=%fused_computation.4 | convolution fusion | flops 2952790016 | bytes 10747904 | tf_op jit(solution)/shard_map/dot_general | solution.py:36
  169.3 17.0 %all-gather.11.cloned.1.call-done = bf16[1408,2048]{1,0:T(8,128)(2,1)} async-done(((bf16[1408,256]{1,0:T(8,128)(2,1)}), bf16[1408,2048]{1,0:T(8,128)(2,1)}) %all-gather.11.cloned.1.call-update) | async-done | bytes 5767184 | tf_op jit(solution)/shard_map/all_gather | solution.py:30
  186.3 7.6 %fusion.3 = f32[512,1408]{1,0:T(8,128)} fusion(bf16[512,2048]{1,0:T(8,128)(2,1)S(1)} %copy-done.1, bf16[1408,2048]{1,0:T(8,128)(2,1)} %all-gather.11.cloned.1.call-done), kind=kOutput, calls=%fused_computation.25 | convolution fusion | flops 2952790016 | bytes 10747904 | tf_op jit(solution)/shard_map/dot_general | solution.py:35
  193.9 14.6 %all-gather.5.cloned.1.call-done = bf16[512,2048]{1,0:T(8,128)(2,1)} async-done(((bf16[128,2048]{1,0:T(8,128)(2,1)}), bf16[512,2048]{1,0:T(8,128)(2,1)}) %all-gather.5.cloned.1.call-update) | async-done | bytes 2097168 | tf_op jit(solution)/shard_map/all_gather | solution.py:27
  208.5 95.1 %all-gather.7.cloned.1.call-done = bf16[1408,2048]{1,0:T(8,128)(2,1)} async-done(((bf16[1408,256]{1,0:T(8,128)(2,1)}), bf16[1408,2048]{1,0:T(8,128)(2,1)}) %all-gather.7.cloned.1.call-update) | async-done | bytes 5767184 | tf_op jit(solution)/shard_map/all_gather | solution.py:32
  303.6 9.1 %multiply_convert_fusion.4 = (bf16[512,1408]{1,0:T(8,128)(2,1)S(1)}, bf16[512,1408]{1,0:T(8,128)(2,1)S(1)}) fusion(f32[512,1408]{1,0:T(8,128)} %fusion.3, f32[512,1408]{1,0:T(8,128)} %convolution_bitcast_fusion, bf16[512,2048]{1,0:T(8,128)(2,1)} %all-gather.5.cloned.1.call-done, bf16[1408,2048]{1,0:T(8,128)(2,1)} %all-gather.7.cloned.1.call-done), kind=kOutput, calls=%fused_computation.6 | convolution fusion | flops 2962161664 | bytes 16515072 | tf_op jit(solution)/shard_map/dot_general | solution.py:37
  313.8 5.0 multiply_convert_fusion.2
  319.0 5.0 multiply_convert_fusion.1
  325.7 8.0 %multiply_convert_fusion = bf16[1408,2048]{1,0:T(8,128)(2,1)} fusion(bf16[512,2048]{1,0:T(8,128)(2,1)S(1)} %copy-done.2, f32[512,1408]{1,0:T(8,128)} %convolution_bitcast_fusion, f32[512,1408]{1,0:T(8,128)} %fusion.3), kind=kOutput, calls=%fused_computation | convolution fusion | flops 2962882560 | bytes 13631488 | tf_op jit(solution)/shard_map/dot_general | solution.py:55
  335.0 5.4 fusion.4
  340.4 7.4 %add_convert_fusion = bf16[512,2048]{1,0:T(8,128)(2,1)} fusion(f32[512,2048]{1,0:T(8,128)S(1)} %fusion.4, bf16[512,1408]{1,0:T(8,128)(2,1)S(1)} %get-tuple-element.16, bf16[1408,2048]{1,0:T(8,128)(2,1)} %constant_dynamic-update-slice_fusion), kind=kOutput, calls=%fused_computation.3 | convolution fusion | flops 2954887168 | bytes 13500416 | tf_op jit(solution)/shard_map/dot_general | solution.py:45
  347.9 80.2 %reduce-scatter.7.cloned.1.call-done = bf16[1408,256]{1,0:T(8,128)(2,1)} async-done(((bf16[1408,2048]{1,0:T(8,128)(2,1)}), bf16[1408,256]{1,0:T(8,128)(2,1)}) %reduce-scatter.7.cloned.1.call-update) | async-done | bytes 720912 | tf_op jit(solution)/shard_map/reduce_scatter | solution.py:57
  430.5 111.6 %reduce-scatter.9.cloned.1.call-done = bf16[1408,256]{1,0:T(8,128)(2,1)} async-done(((bf16[1408,2048]{1,0:T(8,128)(2,1)}), bf16[1408,256]{1,0:T(8,128)(2,1)}) %reduce-scatter.9.cloned.1.call-update) | async-done | bytes 720912 | tf_op jit(solution)/shard_map/reduce_scatter | solution.py:60
  544.4 111.7 %reduce-scatter.11.cloned.1.call-done = bf16[1408,256]{1,0:T(8,128)(2,1)} async-done(((bf16[1408,2048]{1,0:T(8,128)(2,1)}), bf16[1408,256]{1,0:T(8,128)(2,1)}) %reduce-scatter.11.cloned.1.call-update) | async-done | bytes 720912 | tf_op jit(solution)/shard_map/reduce_scatter | solution.py:63
  658.5 35.5 %all-reduce = (f32[1408]{0:T(1024)S(1)}, f32[1408]{0:T(1024)S(1)}, f32[1408]{0:T(1024)S(1)}) all-reduce(f32[1408]{0:T(1024)S(1)} %get-tuple-element.14, f32[1408]{0:T(1024)S(1)} %get-tuple-element.12, f32[1408]{0:T(1024)S(1)} %get-tuple-element.10), channel_id=1, replica_groups=mesh['fs'=8,'tp'=4] {'fs'}, use_global_device_ids=true, to_apply=%region_5.6 | all-reduce | flops 4224 | bytes 33792 | tf_op jit(solution)/shard_map/psum | solution.py:67
  (47 shorter events, 31.1 us)
Async XLA Ops:
  7.2 153.7 %all-gather.9.cloned.1.call-start = ((), (), s32[]{:S(2)}) async-start(), calls=%async_computation.6 | async-start | bytes 2621440 | tf_op jit(solution)/shard_map/all_gather | solution.py:26
  7.9 178.4 %all-gather.11.cloned.1.call-start = ((), (), s32[]{:S(2)}) async-start(), calls=%async_computation.7 | async-start | bytes 6488064 | tf_op jit(solution)/shard_map/all_gather | solution.py:30
  8.7 199.9 %all-gather.5.cloned.1.call-start = ((), (), s32[]{:S(2)}) async-start(), calls=%async_computation.4 | async-start | bytes 2621440 | tf_op jit(solution)/shard_map/all_gather | solution.py:27
  9.4 294.2 %all-gather.7.cloned.1.call-start = ((), (), s32[]{:S(2)}) async-start(), calls=%async_computation.5 | async-start | bytes 6488064 | tf_op jit(solution)/shard_map/all_gather | solution.py:32
  10.0 418.2 %reduce-scatter.7.cloned.1.call-start = ((), (), s32[]{:S(2)}) async-start(), calls=%async_computation.9 | async-start | bytes 6488064 | tf_op jit(solution)/shard_map/reduce_scatter | solution.py:57
  10.0 34.2 %collective-permute-start = (bf16[1408,256]{1,0:T(8,128)(2,1)}, bf16[1408,256]{1,0:T(8,128)(2,1)S(1)}, u32[]{:S(2)}, u32[]{:S(2)}) collective-permute-start(bf16[1408,256]{1,0:T(8,128)(2,1)} %param.7), channel_id=1, source_target_pairs={{0,4},{4,8},{8,12},{12,16},{16,20},{20,24},{24,28},{28,0},{1,5},{5... | collective-permute-start | bytes 2162696 | tf_op jit(solution)/shard_map/ppermute | solution.py:14
  13.0 33.5 %collective-permute-start.1 = (bf16[1408,256]{1,0:T(8,128)(2,1)}, bf16[1408,256]{1,0:T(8,128)(2,1)S(1)}, u32[]{:S(2)}, u32[]{:S(2)}) collective-permute-start(bf16[1408,256]{1,0:T(8,128)(2,1)} %param.7), channel_id=1, source_target_pairs={{0,28},{4,0},{8,4},{12,8},{16,12},{20,16},{24,20},{28,24},{1,29},{... | collective-permute-start | bytes 2162696 | tf_op jit(solution)/shard_map/ppermute | solution.py:17
  44.2 40.0 %collective-permute-start.2 = (bf16[1408,256]{1,0:T(8,128)(2,1)S(1)}, bf16[1408,256]{1,0:T(8,128)(2,1)S(1)}, u32[]{:S(2)}, u32[]{:S(2)}) collective-permute-start(bf16[1408,256]{1,0:T(8,128)(2,1)S(1)} %collective-permute-done), channel_id=1, source_target_pairs={{0,4},{4,8},{8,12},{12,16},{16,20},{20,24},{24,28},{28,0},{1,5},{5... | collective-permute-start | bytes 2162696 | tf_op jit(solution)/shard_map/ppermute | solution.py:14
  46.6 6.3 copy-start
  46.6 42.1 %collective-permute-start.3 = (bf16[1408,256]{1,0:T(8,128)(2,1)S(1)}, bf16[1408,256]{1,0:T(8,128)(2,1)S(1)}, u32[]{:S(2)}, u32[]{:S(2)}) collective-permute-start(bf16[1408,256]{1,0:T(8,128)(2,1)S(1)} %collective-permute-done.1), channel_id=1, source_target_pairs={{0,28},{4,0},{8,4},{12,8},{16,12},{20,16},{24,20},{28,24},{1,29},{... | collective-permute-start | bytes 2162696 | tf_op jit(solution)/shard_map/ppermute | solution.py:17
  84.2 41.6 %collective-permute-start.4 = (bf16[1408,256]{1,0:T(8,128)(2,1)S(1)}, bf16[1408,256]{1,0:T(8,128)(2,1)S(1)}, u32[]{:S(2)}, u32[]{:S(2)}) collective-permute-start(bf16[1408,256]{1,0:T(8,128)(2,1)S(1)} %collective-permute-done.2), channel_id=1, source_target_pairs={{0,4},{4,8},{8,12},{12,16},{16,20},{20,24},{24,28},{28,0},{1,5},{5... | collective-permute-start | bytes 2162696 | tf_op jit(solution)/shard_map/ppermute | solution.py:14
  88.6 42.4 %collective-permute-start.5 = (bf16[1408,256]{1,0:T(8,128)(2,1)S(1)}, bf16[1408,256]{1,0:T(8,128)(2,1)S(1)}, u32[]{:S(2)}, u32[]{:S(2)}) collective-permute-start(bf16[1408,256]{1,0:T(8,128)(2,1)S(1)} %collective-permute-done.3), channel_id=1, source_target_pairs={{0,28},{4,0},{8,4},{12,8},{16,12},{20,16},{24,20},{28,24},{1,29},{... | collective-permute-start | bytes 2162696 | tf_op jit(solution)/shard_map/ppermute | solution.py:17
  125.9 34.0 %collective-permute-start.6 = (bf16[1408,256]{1,0:T(8,128)(2,1)S(1)}, bf16[1408,256]{1,0:T(8,128)(2,1)S(1)}, u32[]{:S(2)}, u32[]{:S(2)}) collective-permute-start(bf16[1408,256]{1,0:T(8,128)(2,1)S(1)} %collective-permute-done.4), channel_id=1, source_target_pairs={{0,4},{4,8},{8,12},{12,16},{16,20},{20,24},{24,28},{28,0},{1,5},{5... | collective-permute-start | bytes 2162696 | tf_op jit(solution)/shard_map/ppermute | solution.py:14
  160.8 25.5 %copy-start.1 = (bf16[512,2048]{1,0:T(8,128)(2,1)S(1)}, bf16[512,2048]{1,0:T(8,128)(2,1)}, u32[]{:S(2)}) copy-start(bf16[512,2048]{1,0:T(8,128)(2,1)} %all-gather.9.cloned.1.call-done) | copy-start | bytes 6291460
  312.7 1.1 copy-start.3
  318.8 223.3 %reduce-scatter.9.cloned.1.call-start = ((), (), s32[]{:S(2)}) async-start(), calls=%async_computation.10 | async-start | bytes 6488064 | tf_op jit(solution)/shard_map/reduce_scatter | solution.py:60
  324.0 1.7 copy-start.2
  324.0 332.1 %reduce-scatter.11.cloned.1.call-start = ((), (), s32[]{:S(2)}) async-start(), calls=%async_computation.11 | async-start | bytes 6488064 | tf_op jit(solution)/shard_map/reduce_scatter | solution.py:63
  333.7 1.4 copy-start.4
  333.7 361.5 %reduce-scatter.5.cloned.1.call-start = ((), (), s32[]{:S(2)}) async-start(), calls=%async_computation.8 | async-start | bytes 2621440 | tf_op jit(solution)/shard_map/reduce_scatter | solution.py:44
Sparse Core Ops, SparseCore 0:
  9.5 25.2 all-gather.8
  36.9 149.3 all-gather.10
  187.8 20.6 all-gather.4
  210.4 93.1 all-gather.6
  318.9 109.1 reduce-scatter.6
  431.6 110.3 reduce-scatter.8
  545.7 110.3 reduce-scatter.10
  659.2 30.5 reduce-scatter.4
